TPU v7x, 512 devices: a 8x2x16 block of a 8x8x16 slice. The times are simulated.
512 devices in a mesh: grp: 2 (over y), ep: 32 (over z, core), tp: 8 (over x).
Axes of the slice: x: 8, y: 2, z: 16, core: 2. Of those that a mesh axis runs over, the one named last changes fastest.
The devices are a block of a 8x8x16 slice.
Arguments:
- tokens: bfloat16 [16384, 2048], P(('grp', 'ep'), 'tp'), parts along dimension 0, may hold values from -6 to 6
- norm_gain: float32 [2048], replicated, may hold values from 0.1 to 1.9
- expert_ids: int32 [16384, 2], P(('grp', 'ep')), parts along dimension 0, may hold values from 0 to 31, all different within a row; in each aligned block of 256 rows (0 to 255, 256 to 511, ...) at most 24 rows name the same one
- gate_weights: float32 [16384, 2], P(('grp', 'ep')), parts along dimension 0, may hold values from 0.25 to 1
- w_gate: bfloat16 [32, 2048, 3072], P('ep', None, 'tp'), may hold values from -0.125 to 0.125
- w_up: bfloat16 [32, 2048, 3072], P('ep', None, 'tp'), may hold values from -0.125 to 0.125
- w_down: bfloat16 [32, 3072, 2048], P('ep', 'tp'), may hold values from -0.15625 to 0.15625
Outputs:
- mixed: bfloat16 [16384, 2048], P(('grp', 'ep'), 'tp'), parts along dimension 0
There are 2 independent parts, one for each index of `grp`. A program takes and returns all parts, laid end to end along the dimension named above; an argument that names none is the same for every part. Nothing has to cross between parts.
Inputs may be any that keep to these rules, and one draw needn't show every extreme that they name: `expert_ids`: each token names 2 different experts. Within the 256 rows of one index of ep (aligned blocks) no expert is named more than 24 times, and in some blocks one expert is named exactly 24 times.
All inputs are finite; a program needn't handle non-finite values.
Results may differ from a plain program's by a relative error of at most 0.015.
Values may be sent and summed in bfloat16 or wider, within the bound.
A program may use at most 64 MiB of HBM per device.

v0:
```python
import jax
import jax.numpy as jnp
from jax import lax
from jax.sharding import Mesh
from jax.sharding import PartitionSpec as P

EP = ("ep_0", "ep_1")
GRP_EP = ("grp", "ep_0", "ep_1")
epsilon = 1e-06


def sent_to_all(array, axis):
    count = lax.axis_size(axis)
    return lax.all_to_all(
        jnp.broadcast_to(array[None], (count, *array.shape)), axis, 0, 0, tiled=True
    )


def over_copies(array, axis):
    everything = sent_to_all(array, axis)
    return jnp.sum(everything, axis=0)


def in_blocks(array, dim, count):
    dims = array.shape
    blocks = array.reshape(*dims[:dim], count, dims[dim] // count, *dims[dim + 1 :])
    return jnp.moveaxis(blocks, dim, 0)


def joined_along(blocks, dim):
    dims = list(blocks.shape[1:])
    dims[dim] *= blocks.shape[0]
    return jnp.moveaxis(blocks, 0, dim).reshape(dims)


def moved_by_axis(blocks, axes, order):
    inside = blocks.shape[1:]
    whole = blocks.reshape(*(lax.axis_size(a) for a in axes), *inside)
    for k in order:
        whole = lax.all_to_all(whole, axes[k], k, k, tiled=True)
    return whole.reshape(-1, *inside)


def core_and_chips(array, groups, order, split_dim, concat_dim):
    count = lax.axis_size(groups[0]) * lax.axis_size(groups[1])
    blocks = in_blocks(array, split_dim, count)
    return joined_along(moved_by_axis(blocks, groups, order), concat_dim)


def on_device(tokens, norm_gain, expert_ids, gate_weights, w_gate, w_up, w_down):
    tok_count = tokens.shape[0]
    top_count = expert_ids.shape[1]
    expert_count = lax.axis_size(EP)
    capacity = 3 * tok_count * top_count // (2 * expert_count)
    model_width = norm_gain.shape[0]
    flat_ids = expert_ids.reshape(-1)
    onehot = (flat_ids[:, None] == jnp.arange(expert_count, dtype=jnp.int32)[None, :]).astype(
        jnp.int32
    )
    earlier = jnp.cumsum(onehot, axis=0) - onehot
    slot_index = jnp.sum(earlier * onehot, axis=1)
    dest_index = flat_ids * capacity + slot_index
    owner_index = jnp.arange(tok_count * top_count, dtype=jnp.int32) // top_count
    slot_token = (
        jnp.full((expert_count * capacity,), tok_count, jnp.int32).at[dest_index].set(owner_index)
    )
    tok_values = tokens.astype(jnp.float32)
    square_sum = over_copies(jnp.sum(tok_values * tok_values, axis=1, keepdims=True), "tp")
    col_count = tokens.shape[1]
    gain_part = lax.dynamic_slice_in_dim(norm_gain, lax.axis_index("tp") * col_count, col_count)
    normed = (tok_values * lax.rsqrt(square_sum / model_width + epsilon) * gain_part).astype(
        jnp.bfloat16
    )
    buffer = jnp.take(normed, slot_token, axis=0, mode="fill", fill_value=0).reshape(
        expert_count, capacity, -1
    )
    received = core_and_chips(buffer, ("ep_0", "ep_1"), (1, 0), 0, 0)
    source_count, item_count, col_count = received.shape
    tok_rows = received.reshape(-1, col_count)
    col_piece = lax.all_gather(tok_rows, "tp", axis=1, tiled=True)
    gate_rows = w_gate[0]
    up_rows = w_up[0]
    gate_part = jnp.dot(col_piece, gate_rows, preferred_element_type=jnp.float32)
    up_part = jnp.dot(col_piece, up_rows, preferred_element_type=jnp.float32)
    hidden = (jax.nn.silu(gate_part) * up_part).astype(jnp.bfloat16)
    partial_value = jnp.dot(hidden, w_down[0], preferred_element_type=jnp.float32)
    partial_value = partial_value.reshape(source_count, item_count, -1)
    summed = lax.psum_scatter(
        partial_value.astype(jnp.bfloat16), "tp", scatter_dimension=2, tiled=True
    )
    came_back = lax.all_to_all(summed, EP, split_axis=0, concat_axis=0, tiled=True)
    picked = came_back.reshape(expert_count * capacity, -1)[dest_index].astype(jnp.float32)
    weighted = picked * gate_weights.reshape(-1)[:, None]
    return jnp.sum(weighted.reshape(tok_count, top_count, -1), axis=1).astype(jnp.bfloat16)


def solution(mesh):
    finer = Mesh(
        mesh.devices.reshape(mesh.shape["grp"], 16, 2, mesh.shape["tp"]),
        ("grp", "ep_0", "ep_1", "tp"),
    )
    in_specs = (
        P(GRP_EP, "tp"),
        P(),
        P(GRP_EP, None),
        P(GRP_EP, None),
        P(EP, None, "tp"),
        P(EP, None, "tp"),
        P(EP, "tp", None),
    )
    out_specs = P(GRP_EP, "tp")
    return jax.shard_map(
        on_device, mesh=finer, in_specs=in_specs, out_specs=out_specs, check_vma=False
    )
```

profile of v0, /device:TPU:65, one launch (start us, length us, event | category | flops | bytes accessed | tf_op | source)
XLA Modules:
  0.0 271.2 jit_solution(14151282188558710371)
XLA Ops:
  6.6 1.1 fusion.11
  7.7 0.6 broadcast_in_dim.29
  8.3 7.9 %all-to-all-start = ((f32[8,256,1]{1,2,0:T(1,128)}), f32[8,256,1]{1,2,0:T(1,128)S(1)}, u32[]{:S(2)}, u32[]{:S(2)}) async-start(f32[8,256,1]{1,2,0:T(1,128)} %broadcast_in_dim.29), calls=%async_computation | async-start | bytes 16384 | tf_op jit(solution)/shard_map/all_to_all | solution.py:14
  16.2 0.8 copy.15
  17.3 0.7 broadcast_multiply_fusion
  18.0 1.2 reduce-window.6
  19.2 0.2 slice_reduce_fusion
  19.9 2.4 scatter_custom_fusion
  22.5 0.8 dynamic_slice.3
  23.3 1.0 fusion.13
  24.3 2.7 gather_fusion
  27.0 0.2 copy_select_fusion
  27.2 41.3 %all_to_all.20 = bf16[16,2,1,24,256]{4,3,0,2,1:T(8,128)(2,1)S(1)} all-to-all(bf16[16,2,1,24,256]{4,3,0,2,1:T(8,128)(2,1)S(1)} %copy_select_fusion), channel_id=1, replica_groups=mesh['grp'=2,'ep_0'=16,'ep_1'=2,'tp'=8] {'ep_1'}, dimensions={1} | all-to-all | bytes 786432 | tf_op jit(solution)/shard_map/all_to_all | solution.py:40
  68.5 24.6 %all_to_all.21 = bf16[16,2,1,24,256]{4,3,1,2,0:T(8,128)(2,1)} all-to-all(bf16[16,2,1,24,256]{4,3,1,2,0:T(8,128)(2,1)S(1)} %copy.20), channel_id=1, replica_groups=mesh['grp'=2,'ep_0'=16,'ep_1'=2,'tp'=8] {'ep_0'}, dimensions={0} | all-to-all | bytes 786432 | tf_op jit(solution)/shard_map/all_to_all | solution.py:40
  93.3 59.5 %all-gather.2.cloned.1.call-done = bf16[768,2048]{1,0:T(8,128)(2,1)} async-done(((bf16[768,256]{1,0:T(8,128)(2,1)}), bf16[768,2048]{1,0:T(8,128)(2,1)}) %all-gather.2.cloned.1.call-update) | async-done | bytes 3145744 | tf_op jit(solution)/shard_map/all_gather | solution.py:80
  152.8 3.8 %fusion.3 = f32[768,384]{1,0:T(8,128)S(1)} fusion(bf16[768,2048]{1,0:T(8,128)(2,1)} %all-gather.2.cloned.1.call-done, bf16[1,2048,384]{2,1,0:T(8,128)(2,1)S(1)} %copy-done.3), kind=kOutput, calls=%fused_computation.7 | convolution fusion | flops 1207959552 | bytes 5898240 | tf_op jit(solution)/shard_map/dot_general | solution.py:83
  156.6 1.8 fusion.8
  158.5 3.5 %convolution_convert_fusion = bf16[32,24,2048]{2,1,0:T(8,128)(2,1)} fusion(bf16[32,24,384]{2,1,0:T(8,128)(2,1)S(1)} %bitcast.48, bf16[1,384,2048]{2,1,0:T(8,128)(2,1)S(1)} %copy-done), kind=kOutput, calls=%fused_computation.3 | convolution fusion | flops 1209532416 | bytes 5308416 | tf_op jit(solution)/shard_map/dot_general | solution.py:86
  162.0 54.2 %reduce-scatter.2.cloned.1.call-done = bf16[32,24,256]{2,1,0:T(8,128)(2,1)} async-done(((bf16[32,24,2048]{2,1,0:T(8,128)(2,1)}), bf16[32,24,256]{2,1,0:T(8,128)(2,1)}) %reduce-scatter.2.cloned.1.call-update) | async-done | bytes 393232 | tf_op jit(solution)/shard_map/reduce_scatter | solution.py:88
  216.2 16.9 %all-to-all-start.3 = ((bf16[32,24,256]{2,1,0:T(8,128)(2,1)}), bf16[32,24,256]{2,1,0:T(8,128)(2,1)S(1)}, u32[]{:S(2)}, u32[]{:S(2)}) async-start(bf16[32,24,256]{2,1,0:T(8,128)(2,1)} %reduce-scatter.2.cloned.1.call-done), calls=%async_computation.4 | async-start | bytes 786432 | tf_op jit(solution)/shard_map/all_to_all | solution.py:91
  233.3 27.4 %all-to-all-done.3 = bf16[32,24,256]{2,1,0:T(8,128)(2,1)S(1)} async-done(((bf16[32,24,256]{2,1,0:T(8,128)(2,1)}), bf16[32,24,256]{2,1,0:T(8,128)(2,1)S(1)}, u32[]{:S(2)}, u32[]{:S(2)}) %all-to-all-start.3) | async-done | bytes 393248 | tf_op jit(solution)/shard_map/all_to_all | solution.py:91
  260.7 1.9 gather_fusion.1
  262.7 0.3 reshape.98
  262.9 1.4 multiply_reduce_fusion
  (35 shorter events, 1.3 us)
Async XLA Ops:
  6.5 152.0 %copy-start = (bf16[1,384,2048]{2,1,0:T(8,128)(2,1)S(1)}, bf16[1,384,2048]{2,1,0:T(8,128)(2,1)}, u32[]{:S(2)}) copy-start(bf16[1,384,2048]{2,1,0:T(8,128)(2,1)} %param.13) | copy-start | bytes 4718596
  8.3 15.0 %all-to-all-start = ((f32[8,256,1]{1,2,0:T(1,128)}), f32[8,256,1]{1,2,0:T(1,128)S(1)}, u32[]{:S(2)}, u32[]{:S(2)}) async-start(f32[8,256,1]{1,2,0:T(1,128)} %broadcast_in_dim.29), calls=%async_computation | async-start | bytes 16384 | tf_op jit(solution)/shard_map/all_to_all | solution.py:14
  16.2 136.6 %all-gather.2.cloned.1.call-start = ((), (), s32[]{:S(2)}) async-start(), calls=%async_computation.5 | async-start | bytes 3538944 | tf_op jit(solution)/shard_map/all_gather | solution.py:80
  27.1 125.6 %copy-start.3 = (bf16[1,2048,384]{2,1,0:T(8,128)(2,1)S(1)}, bf16[1,2048,384]{2,1,0:T(8,128)(2,1)}, u32[]{:S(2)}) copy-start(bf16[1,2048,384]{2,1,0:T(8,128)(2,1)} %param.11) | copy-start | bytes 4718596
  93.2 123.0 %reduce-scatter.2.cloned.1.call-start = ((), (), s32[]{:S(2)}) async-start(), calls=%async_computation.6 | async-start | bytes 3538944 | tf_op jit(solution)/shard_map/reduce_scatter | solution.py:88
  152.8 3.8 %copy-start.2 = (bf16[768,2048]{1,0:T(8,128)(2,1)S(1)}, bf16[768,2048]{1,0:T(8,128)(2,1)}, u32[]{:S(2)}) copy-start(bf16[768,2048]{1,0:T(8,128)(2,1)} %all-gather.2.cloned.1.call-done) | copy-start | bytes 9437188
  152.8 3.8 %copy-start.4 = (bf16[1,2048,384]{2,1,0:T(8,128)(2,1)S(1)}, bf16[1,2048,384]{2,1,0:T(8,128)(2,1)}, u32[]{:S(2)}) copy-start(bf16[1,2048,384]{2,1,0:T(8,128)(2,1)} %param.12) | copy-start | bytes 4718596
  162.0 71.2 %copy-start.1 = (f32[256,2]{0,1:T(2,128)S(1)}, f32[256,2]{0,1:T(2,128)}, u32[]{:S(2)}) copy-start(f32[256,2]{0,1:T(2,128)} %param.10) | copy-start | bytes 6148
  216.2 44.5 %all-to-all-start.3 = ((bf16[32,24,256]{2,1,0:T(8,128)(2,1)}), bf16[32,24,256]{2,1,0:T(8,128)(2,1)S(1)}, u32[]{:S(2)}, u32[]{:S(2)}) async-start(bf16[32,24,256]{2,1,0:T(8,128)(2,1)} %reduce-scatter.2.cloned.1.call-done), calls=%async_computation.4 | async-start | bytes 786432 | tf_op jit(solution)/shard_map/all_to_all | solution.py:91
Sparse Core Ops, SparseCore 0:
  93.3 59.4 all-gather.1
  162.2 54.0 reduce-scatter.1
where the time goes:
time: 272 us; the launch traced here: 271 us
  waiting for transfers between devices  141 us (52%)
  blocking collectives  65.9 us (24%)
  starting transfers between devices  24.9 us (9%)
  between operations  13.6 us (5%)
  local copies, waits for them, and re-layouts  10.6 us (4%)
  matrix products  9.14 us (3%)
  other arithmetic  5.77 us (2%)
    all_to_all x2, blocking collectives, moved_by_axis(): whole = lax.all_to_all(whole, axes[k], k, k, tiled=True)  65.9 us
    all_gather x1, waiting for transfers between devices, on_device(): col_piece = lax.all_gather(tok_rows, 'tp', axis=1, tiled=True)  59.5 us
    reduce_scatter x1, waiting for transfers between devices, on_device(): lax.psum_scatter(partial_value.astype(jnp.bfloat16), 'tp', scatter_dimens...  54.2 us
    all_to_all x1, waiting for transfers between devices, on_device(): lax.all_to_all(summed, EP, split_axis=0, concat_axis=0, tiled=True)  27.4 us
    all_to_all x1, starting transfers between devices, on_device(): lax.all_to_all(summed, EP, split_axis=0, concat_axis=0, tiled=True)  16.9 us
    all_to_all x1, starting transfers between devices, sent_to_all(): lax.all_to_all(jnp.broadcast_to(array[None], (count, *array.shape)), axis...  7.86 us
  transfers between devices with their start and end apart: 4, of which 3 were waited for; matrix products, arithmetic and copies ran while one was open for 3% of the time, Pallas kernels for 0%

commit v1 on v0

--- a/solution.py
+++ b/solution.py
@@ -77,7 +77,9 @@
     received = core_and_chips(buffer, ("ep_0", "ep_1"), (1, 0), 0, 0)
     source_count, item_count, col_count = received.shape
     tok_rows = received.reshape(-1, col_count)
-    col_piece = lax.all_gather(tok_rows, "tp", axis=1, tiled=True)
+    col_piece = jnp.concatenate(
+        lax.all_to_all(jnp.stack([tok_rows] * lax.axis_size("tp")), "tp", 0, 0), axis=1
+    )
     gate_rows = w_gate[0]
     up_rows = w_up[0]
     gate_part = jnp.dot(col_piece, gate_rows, preferred_element_type=jnp.float32)

time: 272 us -> 284 us (1.044)
  blocking collectives: 65.9 us -> 137 us
  waiting for transfers between devices: 141 us -> 84.1 us
    all_to_all x0 -> x1, blocking collectives: none -> 71.4 us  [on_device(): lax.all_to_all(jnp.stack([tok_rows] * lax.axis_size('tp')), 'tp', 0, 0)]
    all_gather x1 -> x0, waiting for transfers between devices: 59.5 us -> none  [on_device(): col_piece = lax.all_gather(tok_rows, 'tp', axis=1, tiled=True)]
  transfers between devices with their start and end apart: 4 -> 3, of which waited for: 3 -> 2; matrix products, arithmetic and copies ran while one was open for 3% -> 3% of each run, Pallas kernels for 0% -> 0%
where the time goes in v1:
time: 284 us; the launch traced here: 283 us
  blocking collectives  137 us (48%)
  waiting for transfers between devices  84.1 us (30%)
  starting transfers between devices  24.7 us (9%)
  between operations  13.6 us (5%)
  local copies, waits for them, and re-layouts  10.9 us (4%)
  matrix products  7.16 us (3%)
  other arithmetic  5.77 us (2%)
    all_to_all x1, blocking collectives, on_device(): lax.all_to_all(jnp.stack([tok_rows] * lax.axis_size('tp')), 'tp', 0, 0)  71.4 us
    all_to_all x2, blocking collectives, moved_by_axis(): whole = lax.all_to_all(whole, axes[k], k, k, tiled=True)  65.7 us
    reduce_scatter x1, waiting for transfers between devices, on_device(): lax.psum_scatter(partial_value.astype(jnp.bfloat16), 'tp', scatter_dimens...  56.7 us
    all_to_all x1, waiting for transfers between devices, on_device(): lax.all_to_all(summed, EP, split_axis=0, concat_axis=0, tiled=True)  27.4 us
    all_to_all x1, starting transfers between devices, on_device(): lax.all_to_all(summed, EP, split_axis=0, concat_axis=0, tiled=True)  16.8 us
    all_to_all x1, starting transfers between devices, sent_to_all(): lax.all_to_all(jnp.broadcast_to(array[None], (count, *array.shape)), axis...  7.86 us
  transfers between devices with their start and end apart: 3, of which 2 were waited for; matrix products, arithmetic and copies ran while one was open for 3% of the time, Pallas kernels for 0%

profile of v1, /device:TPU:65, one launch (start us, length us, event | category | flops | bytes accessed | tf_op | source)
XLA Modules:
  0.0 283.4 jit_solution(5267630439003754427)
XLA Ops:
  6.6 1.1 fusion.11
  7.7 0.6 broadcast_in_dim.29
  8.3 7.9 %all-to-all-start = ((f32[8,256,1]{1,2,0:T(1,128)}), f32[8,256,1]{1,2,0:T(1,128)S(1)}, u32[]{:S(2)}, u32[]{:S(2)}) async-start(f32[8,256,1]{1,2,0:T(1,128)} %broadcast_in_dim.29), calls=%async_computation | async-start | bytes 16384 | tf_op jit(solution)/shard_map/all_to_all | solution.py:14
  16.2 0.8 copy.16
  17.3 0.7 broadcast_multiply_fusion
  18.0 1.2 reduce-window.6
  19.2 0.2 slice_reduce_fusion
  19.9 2.4 scatter_custom_fusion
  22.5 0.8 dynamic_slice.3
  23.3 1.0 fusion.13
  24.3 2.7 gather_fusion
  27.1 41.2 %all_to_all.25 = bf16[16,2,1,24,256]{4,3,0,2,1:T(8,128)(2,1)S(1)} all-to-all(bf16[16,2,1,24,256]{4,3,0,2,1:T(8,128)(2,1)S(1)} %copy_select_fusion), channel_id=1, replica_groups=mesh['grp'=2,'ep_0'=16,'ep_1'=2,'tp'=8] {'ep_1'}, dimensions={1} | all-to-all | bytes 786432 | tf_op jit(solution)/shard_map/all_to_all | solution.py:40
  68.4 24.5 %all_to_all.26 = bf16[16,2,1,24,256]{4,3,1,2,0:T(8,128)(2,1)S(1)} all-to-all(bf16[16,2,1,24,256]{4,3,1,2,0:T(8,128)(2,1)S(1)} %copy.21), channel_id=1, replica_groups=mesh['grp'=2,'ep_0'=16,'ep_1'=2,'tp'=8] {'ep_0'}, dimensions={0} | all-to-all | bytes 786432 | tf_op jit(solution)/shard_map/all_to_all | solution.py:40
  93.1 0.2 stack.3
  93.3 71.4 %all_to_all.27 = bf16[8,768,256]{1,2,0:T(8,128)(2,1)S(1)} all-to-all(bf16[8,768,256]{1,2,0:T(8,128)(2,1)S(1)} %stack.3), channel_id=1, replica_groups=mesh['grp'=2,'ep_0'=16,'ep_1'=2,'tp'=8] {'tp'}, dimensions={0} | all-to-all | bytes 6291456 | tf_op jit(solution)/shard_map/all_to_all | solution.py:81
  164.6 1.8 fusion.3
  166.5 1.9 fusion.8
  168.4 3.5 %convolution_convert_fusion = bf16[32,24,2048]{2,1,0:T(8,128)(2,1)} fusion(bf16[32,24,384]{2,1,0:T(8,128)(2,1)S(1)} %bitcast.53, bf16[1,384,2048]{2,1,0:T(8,128)(2,1)S(1)} %copy-done), kind=kOutput, calls=%fused_computation.3 | convolution fusion | flops 1209532416 | bytes 5308416 | tf_op jit(solution)/shard_map/dot_general | solution.py:88
  171.9 56.7 %reduce-scatter.2.cloned.1.call-done = bf16[32,24,256]{2,1,0:T(8,128)(2,1)} async-done(((bf16[32,24,2048]{2,1,0:T(8,128)(2,1)}), bf16[32,24,256]{2,1,0:T(8,128)(2,1)}) %reduce-scatter.2.cloned.1.call-update) | async-done | bytes 393232 | tf_op jit(solution)/shard_map/reduce_scatter | solution.py:90
  228.6 16.8 %all-to-all-start.4 = ((bf16[32,24,256]{2,1,0:T(8,128)(2,1)}), bf16[32,24,256]{2,1,0:T(8,128)(2,1)S(1)}, u32[]{:S(2)}, u32[]{:S(2)}) async-start(bf16[32,24,256]{2,1,0:T(8,128)(2,1)} %reduce-scatter.2.cloned.1.call-done), calls=%async_computation.5 | async-start | bytes 786432 | tf_op jit(solution)/shard_map/all_to_all | solution.py:93
  245.6 27.4 %all-to-all-done.4 = bf16[32,24,256]{2,1,0:T(8,128)(2,1)S(1)} async-done(((bf16[32,24,256]{2,1,0:T(8,128)(2,1)}), bf16[32,24,256]{2,1,0:T(8,128)(2,1)S(1)}, u32[]{:S(2)}, u32[]{:S(2)}) %all-to-all-start.4) | async-done | bytes 393248 | tf_op jit(solution)/shard_map/all_to_all | solution.py:93
  272.9 1.9 gather_fusion.1
  274.9 0.3 reshape.108
  275.2 1.4 multiply_reduce_fusion
  (33 shorter events, 1.5 us)
Async XLA Ops:
  6.5 161.8 %copy-start = (bf16[1,384,2048]{2,1,0:T(8,128)(2,1)S(1)}, bf16[1,384,2048]{2,1,0:T(8,128)(2,1)}, u32[]{:S(2)}) copy-start(bf16[1,384,2048]{2,1,0:T(8,128)(2,1)} %param.13) | copy-start | bytes 4718596
  8.3 15.0 %all-to-all-start = ((f32[8,256,1]{1,2,0:T(1,128)}), f32[8,256,1]{1,2,0:T(1,128)S(1)}, u32[]{:S(2)}, u32[]{:S(2)}) async-start(f32[8,256,1]{1,2,0:T(1,128)} %broadcast_in_dim.29), calls=%async_computation | async-start | bytes 16384 | tf_op jit(solution)/shard_map/all_to_all | solution.py:14
  16.2 212.5 %reduce-scatter.2.cloned.1.call-start = ((), (), s32[]{:S(2)}) async-start(), calls=%async_computation.6 | async-start | bytes 3538944 | tf_op jit(solution)/shard_map/reduce_scatter | solution.py:90
  93.3 71.4 %copy-start.1 = (bf16[1,2048,384]{2,1,0:T(8,128)(2,1)S(1)}, bf16[1,2048,384]{2,1,0:T(8,128)(2,1)}, u32[]{:S(2)}) copy-start(bf16[1,2048,384]{2,1,0:T(8,128)(2,1)} %param.11) | copy-start | bytes 4718596
  164.6 1.8 copy-start.3
  171.8 73.6 %copy-start.2 = (f32[256,2]{0,1:T(2,128)S(1)}, f32[256,2]{0,1:T(2,128)}, u32[]{:S(2)}) copy-start(f32[256,2]{0,1:T(2,128)} %param.10) | copy-start | bytes 6148
  228.6 44.3 %all-to-all-start.4 = ((bf16[32,24,256]{2,1,0:T(8,128)(2,1)}), bf16[32,24,256]{2,1,0:T(8,128)(2,1)S(1)}, u32[]{:S(2)}, u32[]{:S(2)}) async-start(bf16[32,24,256]{2,1,0:T(8,128)(2,1)} %reduce-scatter.2.cloned.1.call-done), calls=%async_computation.5 | async-start | bytes 786432 | tf_op jit(solution)/shard_map/all_to_all | solution.py:93
Sparse Core Ops, SparseCore 0:
  172.0 56.5 reduce-scatter.1
